TPU v7x, 32 devices: a whole 2x2x4 slice. The times are simulated.
32 devices in a mesh: kv: 8 (over z, x), tp: 4 (over y, core).
Axes of the slice: x: 2, y: 2, z: 4, core: 2. Of those that a mesh axis runs over, the one named last changes fastest.
Arguments:
- hidden_in: bfloat16 [24, 4096], P('kv'), may hold values from -6 to 6
- norm_gain: float32 [4096], replicated, may hold values from 0.1 to 1.9
- w_query: bfloat16 [4096, 2048], P('kv', 'tp'), may hold values from -0.09375 to 0.09375
- w_key: bfloat16 [4096, 2048], P('kv', 'tp'), may hold values from -0.09375 to 0.09375
- w_value: bfloat16 [4096, 4096], P('kv', 'tp'), may hold values from -0.09375 to 0.09375
- w_out: bfloat16 [4096, 4096], P('kv', 'tp'), may hold values from -0.09375 to 0.09375
- carried_state: float32 [8, 8, 256, 512], P('kv', 'tp'), may hold values from -0.625 to 0.625
- prior_keys: bfloat16 [8, 8, 3, 256], P('kv', 'tp'), may hold values from -0.375 to 0.375
- prior_values: bfloat16 [8, 8, 3, 512], P('kv', 'tp'), may hold values from -6 to 6
- accepted: int32 [8], P('kv'), may hold values from 0 to 3
- lengths: int32 [8], P('kv'), may hold values from 1 to 4096
Outputs:
- layer_out: bfloat16 [24, 4096], P('tp', 'kv')
- committed_state: float32 [8, 8, 256, 512], P('kv', 'tp')
- new_keys: bfloat16 [8, 8, 3, 256], P('kv', 'tp')
- new_values: bfloat16 [8, 8, 3, 512], P('kv', 'tp')
All inputs are finite; a program needn't handle non-finite values.
Results may differ from a plain program's by a relative error of at most 0.014.
Values may be sent and summed in bfloat16 or wider, within the bound.
A program may use at most 64 MiB of HBM per device.

v0:
```python
import jax
import jax.numpy as jnp
from jax import lax
from jax.sharding import PartitionSpec as P

epsilon = 1e-06
rotary_base = 10000.0


def rotate(values, places):
    middle = values.shape[-1] // 2
    inverse = rotary_base ** (-jnp.linspace(0.0, 1.0, middle, dtype=jnp.float32))
    angles = places[..., None] * inverse
    cosine = jnp.cos(angles)[:, :, None, :]
    sine_term = jnp.sin(angles)[:, :, None, :]
    leading = values[..., :middle]
    trailing = values[..., middle:]
    return jnp.concatenate(
        [leading * cosine - trailing * sine_term, leading * sine_term + trailing * cosine], axis=-1
    )


def retain(
    queries,
    key_rows,
    value_rows,
    carried_state,
    prior_keys,
    prior_values,
    accepted,
    lengths,
    head_ids,
):
    steps_ahead = queries.shape[1]
    key_size = queries.shape[-1]
    log_decay = jnp.log(1.0 - 2.0 ** (-5.0 - head_ids))
    slot_ids = jnp.arange(steps_ahead, dtype=jnp.float32)
    places = (lengths + accepted).astype(jnp.float32)[:, None] + slot_ids[None, :]
    turned_q = rotate(queries.astype(jnp.float32), places)
    turned_k = rotate(key_rows.astype(jnp.float32), places) * key_size ** (-0.5)
    taken_count = accepted.astype(jnp.float32)[:, None]
    lag_steps = taken_count[:, :, None] - 1.0 - slot_ids[None, None, :]
    weights_back = jnp.where(
        lag_steps >= 0.0, jnp.exp(log_decay[None, :, None] * jnp.maximum(lag_steps, 0.0)), 0.0
    )
    keep_factor = jnp.exp(log_decay[None, :] * taken_count)
    scaled_keys = prior_keys.astype(jnp.float32) * weights_back[..., None]
    committed = keep_factor[..., None, None] * carried_state + jnp.einsum(
        "shjd,shje->shde",
        scaled_keys,
        prior_values.astype(jnp.float32),
        precision=lax.Precision.HIGHEST,
    )
    reach_decay = jnp.exp(log_decay[None, :] * (slot_ids[:, None] + 1.0))
    carried_part = (
        jnp.einsum("sihd,shde->sihe", turned_q, committed, precision=lax.Precision.HIGHEST)
        * reach_decay[None, :, :, None]
    )
    distance = slot_ids[:, None] - slot_ids[None, :]
    weight = jnp.where(
        distance[None] >= 0.0,
        jnp.exp(log_decay[:, None, None] * jnp.maximum(distance, 0.0)[None]),
        0.0,
    )
    scores = (
        jnp.einsum("sihd,sjhd->shij", turned_q, turned_k, precision=lax.Precision.HIGHEST)
        * weight[None]
    )
    inner_part = jnp.einsum(
        "shij,sjhe->sihe", scores, value_rows.astype(jnp.float32), precision=lax.Precision.HIGHEST
    )
    retained = carried_part + inner_part
    normed = retained * lax.rsqrt(jnp.mean(retained * retained, axis=-1, keepdims=True) + epsilon)
    return (normed.astype(jnp.bfloat16), committed, turned_k)


def body(
    hidden_in,
    norm_gain,
    w_query,
    w_key,
    w_value,
    w_out,
    carried_state,
    prior_keys,
    prior_values,
    accepted,
    lengths,
):
    row_values = hidden_in.astype(jnp.float32)
    normed = (
        row_values
        * lax.rsqrt(jnp.mean(row_values * row_values, axis=-1, keepdims=True) + epsilon)
        * norm_gain
    ).astype(jnp.bfloat16)
    own_rows = normed.shape[0]
    query_width = w_query.shape[1]
    key_width = w_key.shape[1]
    columns = lax.all_to_all(normed, "kv", split_axis=1, concat_axis=0, tiled=True)
    joined = jnp.concatenate((w_query, w_key, w_value), axis=1)
    group_count = lax.axis_size("kv")
    partial_term = jnp.dot(columns, joined, preferred_element_type=jnp.float32)
    grouped = partial_term.reshape(group_count, own_rows, partial_term.shape[1])
    received = lax.all_to_all(grouped, "kv", split_axis=0, concat_axis=0, tiled=True)
    joint_sum = jnp.sum(received, axis=0)
    query_sum = joint_sum[:, :query_width]
    key_sum = joint_sum[:, query_width : query_width + key_width]
    value_sum = joint_sum[:, query_width + key_width :]
    seq_count, head_count, steps_ahead = (
        prior_keys.shape[0],
        prior_keys.shape[1],
        prior_keys.shape[2],
    )

    def by_heads(matrix):
        return matrix.astype(jnp.bfloat16).reshape(seq_count, steps_ahead, head_count, -1)

    value_rows = by_heads(value_sum)
    head_ids = (lax.axis_index("tp") * head_count + jnp.arange(head_count)).astype(jnp.float32)
    heads_out, committed, turned_k = retain(
        by_heads(query_sum),
        by_heads(key_sum),
        value_rows,
        carried_state,
        prior_keys,
        prior_values,
        accepted,
        lengths,
        head_ids,
    )
    flat_rows = heads_out.reshape(own_rows, -1)
    head_terms = lax.dot_general(
        lax.all_gather(flat_rows, "kv", axis=0, tiled=True),
        w_out,
        (((1,), (1,)), ((), ())),
        preferred_element_type=jnp.float32,
    )
    layer_out = lax.psum_scatter(
        head_terms.astype(jnp.bfloat16), "tp", scatter_dimension=0, tiled=True
    )
    new_keys = jnp.transpose(turned_k, (0, 2, 1, 3)).astype(jnp.bfloat16)
    new_values = jnp.transpose(value_rows, (0, 2, 1, 3))
    return (layer_out, committed, new_keys, new_values)


def solution(mesh):
    in_specs = (
        P("kv", None),
        P(),
        P("kv", "tp"),
        P("kv", "tp"),
        P("kv", "tp"),
        P("kv", "tp"),
        P("kv", "tp", None, None),
        P("kv", "tp", None, None),
        P("kv", "tp", None, None),
        P("kv"),
        P("kv"),
    )
    out_specs = (
        P("tp", "kv"),
        P("kv", "tp", None, None),
        P("kv", "tp", None, None),
        P("kv", "tp", None, None),
    )
    return jax.shard_map(body, mesh=mesh, in_specs=in_specs, out_specs=out_specs, check_vma=False)
```

profile of v0, /device:TPU:1, one launch (start us, length us, event | category | flops | bytes accessed | tf_op | source)
XLA Modules:
  0.0 75.8 jit_solution(14520870958238705790)
XLA Ops:
  0.6 0.0 copy-start
  0.6 1.0 %fusion.6 = f32[3]{0:T(128)S(1)} fusion(bf16[3,4096]{1,0:T(4,128)(2,1)} %param.13), kind=kLoop, calls=%fused_computation.13 | loop fusion | flops 36861 | bytes 24588 | tf_op jit(solution)/shard_map/reduce_sum | solution.py:93
  1.6 1.5 %fusion.8 = bf16[3,4096]{1,0:T(4,128)(2,1)} fusion(bf16[3,4096]{1,0:T(4,128)(2,1)} %param.13, f32[4096]{0:T(1024)} %param.14, f32[3]{0:T(128)S(1)} %add_rsqrt_fusion.1), kind=kLoop, calls=%fused_computation.15 | loop fusion | flops 49152 | bytes 65548 | tf_op jit(solution)/shard_map/convert_element_type | solution.py:95
  3.1 6.3 %all-to-all-start = ((bf16[3,8,512]{2,0,1:T(4,128)(2,1)}), bf16[3,8,512]{2,0,1:T(4,128)(2,1)S(1)}, u32[]{:S(2)}, u32[]{:S(2)}) async-start(bf16[3,8,512]{2,0,1:T(4,128)(2,1)} %bitcast.6), calls=%async_computation | async-start | bytes 65536 | tf_op jit(solution)/shard_map/all_to_all | solution.py:99
  10.9 0.1 multiply_exponential_fusion
  10.9 0.1 fusion.20
  11.0 0.1 exponential_select_fusion
  11.1 0.1 multiply_cosine_fusion
  11.2 0.8 %multiply_bitcast_fusion = f32[2,3,256]{2,0,1:T(2,128)S(1)} fusion(bf16[1,2,3,256]{3,1,2,0:T(2,128)(2,1)} %param.20, f32[2,3]{0,1:T(4,128)S(1)} %exponential_select_fusion), kind=kLoop, calls=%fused_computation.28 | loop fusion | flops 3072 | bytes 9240 | tf_op jit(solution)/shard_map/reshape.14
  12.0 1.2 %dynamic-slice.4 = u32[1]{0:T(128)} dynamic-slice(u32[32]{0:T(128)} %constant.49, u32[]{:S(6)} %partition-id.5), dynamic_slice_sizes={1} | dynamic-slice | bytes 12
  13.9 0.0 copy-start.3
  13.9 1.1 %all-to-all-done = bf16[3,8,512]{2,0,1:T(4,128)(2,1)S(1)} async-done(((bf16[3,8,512]{2,0,1:T(4,128)(2,1)}), bf16[3,8,512]{2,0,1:T(4,128)(2,1)S(1)}, u32[]{:S(2)}, u32[]{:S(2)}) %all-to-all-start) | async-done | bytes 24608 | tf_op jit(solution)/shard_map/all_to_all | solution.py:99
  15.0 0.0 copy-start.2
  15.0 2.0 %fusion.1 = f32[8,3,2048]{2,0,1:T(8,128)S(1)} fusion(bf16[512,1024]{1,0:T(8,128)(2,1)} %param.17, bf16[512,512]{1,0:T(8,128)(2,1)} %param.16, bf16[512,512]{1,0:T(8,128)(2,1)} %param.15, bf16[3,8,512]{2,0,1:T(4,128)(2,1)S(1)} %all-to-all-done), kind=kOutput, calls=%fused_computation.1 | convolution fusion | flops 56623104 | bytes 2318336 | tf_op jit(solution)/shard_map/dot_general | solution.py:102
  17.0 0.8 %copy.24 = f32[8,3,2048]{2,1,0:T(4,128)} copy(f32[8,3,2048]{2,0,1:T(8,128)S(1)} %fusion.1) | data formatting | bytes 393216 | tf_op jit(solution)/shard_map/dot_general | solution.py:102
  17.8 4.4 %all-to-all-start.1 = ((f32[8,3,2048]{2,1,0:T(4,128)}), f32[8,3,2048]{2,1,0:T(4,128)S(1)}, u32[]{:S(2)}, u32[]{:S(2)}) async-start(f32[8,3,2048]{2,1,0:T(4,128)} %copy.24), calls=%async_computation.1 | async-start | bytes 524288 | tf_op jit(solution)/shard_map/all_to_all | solution.py:104
  22.2 0.0 copy-done.3
  22.2 0.0 copy-done.2
  22.2 0.7 fusion.2
  22.9 0.0 copy-start.1
  22.9 6.4 %all-to-all-done.1 = f32[8,3,2048]{2,1,0:T(4,128)S(1)} async-done(((f32[8,3,2048]{2,1,0:T(4,128)}), f32[8,3,2048]{2,1,0:T(4,128)S(1)}, u32[]{:S(2)}, u32[]{:S(2)}) %all-to-all-start.1) | async-done | bytes 196640 | tf_op jit(solution)/shard_map/all_to_all | solution.py:104
  29.4 0.1 reduce_sum.28
  29.5 0.1 convolution_multiply_fusion
  29.6 0.1 convolution_bitcast_fusion.1
  29.7 0.7 multiply_reduce_fusion
  30.5 0.1 multiply_convert_fusion
  30.6 24.5 %all-gather = bf16[8,3,1024]{2,1,0:T(4,128)(2,1)S(1)} all-gather(bf16[1,3,1024]{2,1,0:T(4,128)(2,1)S(1)} %bitcast.60), channel_id=1, replica_groups=mesh['kv'=8,'tp'=4] {'kv'}, dimensions={0}, use_global_device_ids=true | all-gather | bytes 55296 | tf_op jit(solution)/shard_map/all_gather | solution.py:133
  55.1 0.0 copy-done
  55.1 0.4 convolution_convert_fusion
  55.5 0.0 copy-done.1
  55.5 14.2 %fusion = bf16[8,512]{1,0:T(8,128)(2,1)S(1)} fusion(bf16[24,512]{1,0:T(8,128)(2,1)S(1)} %convolution_convert_fusion), kind=kCustom, calls=%all-reduce-scatter | all-reduce-scatter fusion | flops 16385 | bytes 33280
  69.7 4.2 %collective-permute-start = (bf16[6,512]{1,0:T(8,128)(2,1)S(1)}, bf16[6,512]{1,0:T(8,128)(2,1)S(1)}, u32[]{:S(2)}, u32[]{:S(2)}) collective-permute-start(bf16[6,512]{1,0:T(8,128)(2,1)S(1)} %slice.38), channel_id=1, source_target_pairs={{0,1},{1,2},{2,3},{4,5},{5,6},{6,7},{8,9},{9,10},{10,11},{12,13},{... | collective-permute-start | bytes 18440
  73.9 0.6 reshape.407
  74.5 0.6 copy.25
  75.1 0.0 collective-permute-done
  75.1 0.1 concatenate.34
  75.2 0.6 constant_dynamic-slice_fusion
  (19 shorter events, 0.2 us)
Async XLA Ops:
  0.6 54.5 %copy-start = (bf16[512,1024]{1,0:T(8,128)(2,1)S(1)}, bf16[512,1024]{1,0:T(8,128)(2,1)}, u32[]{:S(2)}) copy-start(bf16[512,1024]{1,0:T(8,128)(2,1)} %param.18) | copy-start | bytes 3145732
  3.1 11.9 %all-to-all-start = ((bf16[3,8,512]{2,0,1:T(4,128)(2,1)}), bf16[3,8,512]{2,0,1:T(4,128)(2,1)S(1)}, u32[]{:S(2)}, u32[]{:S(2)}) async-start(bf16[3,8,512]{2,0,1:T(4,128)(2,1)} %bitcast.6), calls=%async_computation | async-start | bytes 65536 | tf_op jit(solution)/shard_map/all_to_all | solution.py:99
  13.9 8.3 %copy-start.3 = (bf16[1,2,3,512]{3,1,2,0:T(2,128)(2,1)S(1)}, bf16[1,2,3,512]{3,1,2,0:T(2,128)(2,1)}, u32[]{:S(2)}) copy-start(bf16[1,2,3,512]{3,1,2,0:T(2,128)(2,1)} %param.21) | copy-start | bytes 18436
  15.0 7.2 %copy-start.2 = (f32[1,2,256,512]{3,2,1,0:T(8,128)S(1)}, f32[1,2,256,512]{3,2,1,0:T(8,128)}, u32[]{:S(2)}) copy-start(f32[1,2,256,512]{3,2,1,0:T(8,128)} %param.19) | copy-start | bytes 3145732
  17.8 11.5 %all-to-all-start.1 = ((f32[8,3,2048]{2,1,0:T(4,128)}), f32[8,3,2048]{2,1,0:T(4,128)S(1)}, u32[]{:S(2)}, u32[]{:S(2)}) async-start(f32[8,3,2048]{2,1,0:T(4,128)} %copy.24), calls=%async_computation.1 | async-start | bytes 524288 | tf_op jit(solution)/shard_map/all_to_all | solution.py:104
  22.9 32.6 %copy-start.1 = (f32[1,2,256,512]{3,2,1,0:T(8,128)}, f32[1,2,256,512]{3,2,1,0:T(8,128)S(1)}, u32[]{:S(2)}) copy-start(f32[1,2,256,512]{3,2,1,0:T(8,128)S(1)} %fusion.2) | copy-start | bytes 3145732
  69.7 5.4 %collective-permute-start = (bf16[6,512]{1,0:T(8,128)(2,1)S(1)}, bf16[6,512]{1,0:T(8,128)(2,1)S(1)}, u32[]{:S(2)}, u32[]{:S(2)}) collective-permute-start(bf16[6,512]{1,0:T(8,128)(2,1)S(1)} %slice.38), channel_id=1, source_target_pairs={{0,1},{1,2},{2,3},{4,5},{5,6},{6,7},{8,9},{9,10},{10,11},{12,13},{... | collective-permute-start | bytes 18440
where the time goes:
time: 76.3 us; the launch traced here: 75.8 us
  blocking collectives  38.7 us (51%)
  starting transfers between devices  14.9 us (20%)
  waiting for transfers between devices  7.55 us (10%)
  matrix products  4.06 us (5%)
  local copies, waits for them, and re-layouts  4.05 us (5%)
  other arithmetic  3.82 us (5%)
  between operations  2.77 us (4%)
    all_gather x1, blocking collectives, body(): lax.all_gather(flat_rows, 'kv', axis=0, tiled=True)  24.5 us
    unnamed x1, blocking collectives  14.2 us
    all_to_all x1, waiting for transfers between devices, body(): lax.all_to_all(grouped, 'kv', split_axis=0, concat_axis=0, tiled=True)  6.45 us
    all_to_all x1, starting transfers between devices, body(): lax.all_to_all(normed, 'kv', split_axis=1, concat_axis=0, tiled=True)  6.34 us
    all_to_all x1, starting transfers between devices, body(): lax.all_to_all(grouped, 'kv', split_axis=0, concat_axis=0, tiled=True)  4.36 us
    unnamed x1, starting transfers between devices  4.18 us
    unnamed x14, local copies, waits for them, and re-layouts  2.59 us
    dot_general x1, matrix products, body(): partial_term = jnp.dot(columns, joined, preferred_element_type=jnp.float32)  1.98 us
  transfers between devices with their start and end apart: 3, of which 2 were waited for; matrix products, arithmetic and copies ran while one was open for 6% of the time, Pallas kernels for 0%

commit v1 on v0

--- a/solution.py
+++ b/solution.py
@@ -96,7 +96,10 @@
     own_rows = normed.shape[0]
     query_width = w_query.shape[1]
     key_width = w_key.shape[1]
-    columns = lax.all_to_all(normed, "kv", split_axis=1, concat_axis=0, tiled=True)
+    columns = jnp.concatenate(
+        lax.all_to_all(jnp.stack(jnp.split(normed, lax.axis_size("kv"), axis=1)), "kv", 0, 0),
+        axis=0,
+    )
     joined = jnp.concatenate((w_query, w_key, w_value), axis=1)
     group_count = lax.axis_size("kv")
     partial_term = jnp.dot(columns, joined, preferred_element_type=jnp.float32)

time: 76.3 us -> 80.4 us (1.054)
  local copies, waits for them, and re-layouts: 4.05 us -> 8.82 us
    unnamed x14 -> x21, local copies, waits for them, and re-layouts: 2.59 us -> 6.76 us
  transfers between devices with their start and end apart: 3 -> 3, of which waited for: 2 -> 2; matrix products, arithmetic and copies ran while one was open for 6% -> 5% of each run, Pallas kernels for 0% -> 0%
where the time goes in v1:
time: 80.4 us; the launch traced here: 80 us
  blocking collectives  38.7 us (48%)
  starting transfers between devices  14.9 us (19%)
  local copies, waits for them, and re-layouts  8.82 us (11%)
  waiting for transfers between devices  7.55 us (9%)
  matrix products  4.06 us (5%)
  other arithmetic  3.21 us (4%)
  between operations  2.78 us (3%)
    all_gather x1, blocking collectives, body(): lax.all_gather(flat_rows, 'kv', axis=0, tiled=True)  24.5 us
    unnamed x1, blocking collectives  14.2 us
    unnamed x21, local copies, waits for them, and re-layouts  6.76 us
    all_to_all x1, waiting for transfers between devices, body(): lax.all_to_all(grouped, 'kv', split_axis=0, concat_axis=0, tiled=True)  6.45 us
    all_to_all x1, starting transfers between devices, body(): lax.all_to_all(jnp.stack(jnp.split(normed, lax.axis_size('kv'), axis=1)),...  6.34 us
    all_to_all x1, starting transfers between devices, body(): lax.all_to_all(grouped, 'kv', split_axis=0, concat_axis=0, tiled=True)  4.36 us
    unnamed x1, starting transfers between devices  4.18 us
    dot_general x1, matrix products, body(): partial_term = jnp.dot(columns, joined, preferred_element_type=jnp.float32)  1.98 us
  transfers between devices with their start and end apart: 3, of which 2 were waited for; matrix products, arithmetic and copies ran while one was open for 5% of the time, Pallas kernels for 0%

profile of v1, /device:TPU:1, one launch (start us, length us, event | category | flops | bytes accessed | tf_op | source)
XLA Modules:
  0.0 80.0 jit_solution(15221966568025053566)
XLA Ops:
  0.6 0.0 copy-start
  0.6 1.0 %fusion.6 = f32[3]{0:T(128)S(1)} fusion(bf16[3,4096]{1,0:T(4,128)(2,1)} %param.13), kind=kLoop, calls=%fused_computation.13 | loop fusion | flops 36861 | bytes 24588 | tf_op jit(solution)/shard_map/reduce_sum | solution.py:93
  1.6 0.9 %fusion.8 = bf16[3,4096]{1,0:T(4,128)(2,1)S(1)} fusion(bf16[3,4096]{1,0:T(4,128)(2,1)} %param.13, f32[4096]{0:T(1024)} %param.14, f32[3]{0:T(128)S(1)} %add_rsqrt_fusion.1), kind=kLoop, calls=%fused_computation.15 | loop fusion | flops 49152 | bytes 65548 | tf_op jit(solution)/shard_map/convert_element_type | solution.py:95
  2.5 0.6 constant_dynamic-update-slice_fusion.7
  3.1 0.6 constant_dynamic-update-slice_fusion.6
  3.7 0.6 constant_dynamic-update-slice_fusion.5
  4.3 0.6 constant_dynamic-update-slice_fusion.4
  4.9 0.6 constant_dynamic-update-slice_fusion.3
  5.5 0.6 constant_dynamic-update-slice_fusion.2
  6.1 0.6 constant_dynamic-update-slice_fusion.1
  6.7 0.6 constant_dynamic-update-slice_fusion
  7.3 6.3 %all-to-all-start = ((bf16[8,3,512]{2,1,0:T(4,128)(2,1)}), bf16[8,3,512]{2,1,0:T(4,128)(2,1)S(1)}, u32[]{:S(2)}, u32[]{:S(2)}) async-start(bf16[8,3,512]{2,1,0:T(4,128)(2,1)} %constant_dynamic-update-slice_fusion), calls=%async_computation | async-start | bytes 65536 | tf_op jit(solution)/shard_map/all_to_all | solution.py:100
  15.0 0.1 multiply_exponential_fusion
  15.1 0.1 fusion.19
  15.2 0.1 exponential_select_fusion
  15.3 0.1 multiply_cosine_fusion
  15.4 0.8 multiply_bitcast_fusion
  16.1 1.2 %dynamic-slice.4 = u32[1]{0:T(128)} dynamic-slice(u32[32]{0:T(128)} %constant.49, u32[]{:S(6)} %partition-id.5), dynamic_slice_sizes={1} | dynamic-slice | bytes 12
  18.0 0.0 copy-start.3
  18.1 1.1 %all-to-all-done = bf16[8,3,512]{2,1,0:T(4,128)(2,1)S(1)} async-done(((bf16[8,3,512]{2,1,0:T(4,128)(2,1)}), bf16[8,3,512]{2,1,0:T(4,128)(2,1)S(1)}, u32[]{:S(2)}, u32[]{:S(2)}) %all-to-all-start) | async-done | bytes 24608 | tf_op jit(solution)/shard_map/all_to_all | solution.py:100
  19.2 0.0 copy-start.2
  19.2 2.0 %fusion.1 = f32[8,3,2048]{2,0,1:T(8,128)S(1)} fusion(bf16[512,1024]{1,0:T(8,128)(2,1)} %param.17, bf16[512,512]{1,0:T(8,128)(2,1)} %param.16, bf16[512,512]{1,0:T(8,128)(2,1)} %param.15, bf16[8,3,512]{2,1,0:T(4,128)(2,1)S(1)} %all-to-all-done), kind=kOutput, calls=%fused_computation.1 | convolution fusion | flops 56623104 | bytes 2318336 | tf_op jit(solution)/shard_map/dot_general | solution.py:105
  21.1 0.8 %copy.109 = f32[8,3,2048]{2,1,0:T(4,128)} copy(f32[8,3,2048]{2,0,1:T(8,128)S(1)} %fusion.1) | data formatting | bytes 393216 | tf_op jit(solution)/shard_map/dot_general | solution.py:105
  22.0 4.4 %all-to-all-start.1 = ((f32[8,3,2048]{2,1,0:T(4,128)}), f32[8,3,2048]{2,1,0:T(4,128)S(1)}, u32[]{:S(2)}, u32[]{:S(2)}) async-start(f32[8,3,2048]{2,1,0:T(4,128)} %copy.109), calls=%async_computation.1 | async-start | bytes 524288 | tf_op jit(solution)/shard_map/all_to_all | solution.py:107
  26.3 0.0 copy-done.3
  26.4 0.0 copy-done.2
  26.4 0.7 fusion.2
  27.1 0.0 copy-start.1
  27.1 6.4 %all-to-all-done.1 = f32[8,3,2048]{2,1,0:T(4,128)S(1)} async-done(((f32[8,3,2048]{2,1,0:T(4,128)}), f32[8,3,2048]{2,1,0:T(4,128)S(1)}, u32[]{:S(2)}, u32[]{:S(2)}) %all-to-all-start.1) | async-done | bytes 196640 | tf_op jit(solution)/shard_map/all_to_all | solution.py:107
  33.5 0.1 reduce_sum.28
  33.6 0.1 convolution_multiply_fusion
  33.8 0.1 convolution_bitcast_fusion.1
  33.9 0.7 multiply_reduce_fusion
  34.7 0.1 multiply_convert_fusion
  34.7 24.5 %all-gather = bf16[8,3,1024]{2,1,0:T(4,128)(2,1)S(1)} all-gather(bf16[1,3,1024]{2,1,0:T(4,128)(2,1)S(1)} %bitcast.88), channel_id=1, replica_groups=mesh['kv'=8,'tp'=4] {'kv'}, dimensions={0}, use_global_device_ids=true | all-gather | bytes 55296 | tf_op jit(solution)/shard_map/all_gather | solution.py:136
  59.3 0.0 copy-done
  59.3 0.4 convolution_convert_fusion
  59.7 0.0 copy-done.1
  59.7 14.2 %fusion = bf16[8,512]{1,0:T(8,128)(2,1)S(1)} fusion(bf16[24,512]{1,0:T(8,128)(2,1)S(1)} %convolution_convert_fusion), kind=kCustom, calls=%all-reduce-scatter | all-reduce-scatter fusion | flops 16385 | bytes 33280
  73.9 4.2 %collective-permute-start = (bf16[6,512]{1,0:T(8,128)(2,1)S(1)}, bf16[6,512]{1,0:T(8,128)(2,1)S(1)}, u32[]{:S(2)}, u32[]{:S(2)}) collective-permute-start(bf16[6,512]{1,0:T(8,128)(2,1)S(1)} %slice.38), channel_id=1, source_target_pairs={{0,1},{1,2},{2,3},{4,5},{5,6},{6,7},{8,9},{9,10},{10,11},{12,13},{... | collective-permute-start | bytes 18440
  78.1 0.6 reshape.405
  78.7 0.6 copy.110
  79.3 0.0 collective-permute-done
  79.3 0.1 concatenate.34
  79.3 0.6 constant_dynamic-slice_fusion
  (19 shorter events, 0.2 us)
Async XLA Ops:
  0.6 58.6 %copy-start = (bf16[512,1024]{1,0:T(8,128)(2,1)S(1)}, bf16[512,1024]{1,0:T(8,128)(2,1)}, u32[]{:S(2)}) copy-start(bf16[512,1024]{1,0:T(8,128)(2,1)} %param.18) | copy-start | bytes 3145732
  7.3 11.9 %all-to-all-start = ((bf16[8,3,512]{2,1,0:T(4,128)(2,1)}), bf16[8,3,512]{2,1,0:T(4,128)(2,1)S(1)}, u32[]{:S(2)}, u32[]{:S(2)}) async-start(bf16[8,3,512]{2,1,0:T(4,128)(2,1)} %constant_dynamic-update-slice_fusion), calls=%async_computation | async-start | bytes 65536 | tf_op jit(solution)/shard_map/all_to_all | solution.py:100
  18.0 8.3 %copy-start.3 = (bf16[1,2,3,512]{3,1,2,0:T(2,128)(2,1)S(1)}, bf16[1,2,3,512]{3,1,2,0:T(2,128)(2,1)}, u32[]{:S(2)}) copy-start(bf16[1,2,3,512]{3,1,2,0:T(2,128)(2,1)} %param.21) | copy-start | bytes 18436
  19.2 7.2 %copy-start.2 = (f32[1,2,256,512]{3,2,1,0:T(8,128)S(1)}, f32[1,2,256,512]{3,2,1,0:T(8,128)}, u32[]{:S(2)}) copy-start(f32[1,2,256,512]{3,2,1,0:T(8,128)} %param.19) | copy-start | bytes 3145732
  22.0 11.5 %all-to-all-start.1 = ((f32[8,3,2048]{2,1,0:T(4,128)}), f32[8,3,2048]{2,1,0:T(4,128)S(1)}, u32[]{:S(2)}, u32[]{:S(2)}) async-start(f32[8,3,2048]{2,1,0:T(4,128)} %copy.109), calls=%async_computation.1 | async-start | bytes 524288 | tf_op jit(solution)/shard_map/all_to_all | solution.py:107
  27.1 32.6 %copy-start.1 = (f32[1,2,256,512]{3,2,1,0:T(8,128)}, f32[1,2,256,512]{3,2,1,0:T(8,128)S(1)}, u32[]{:S(2)}) copy-start(f32[1,2,256,512]{3,2,1,0:T(8,128)S(1)} %fusion.2) | copy-start | bytes 3145732
  73.9 5.4 %collective-permute-start = (bf16[6,512]{1,0:T(8,128)(2,1)S(1)}, bf16[6,512]{1,0:T(8,128)(2,1)S(1)}, u32[]{:S(2)}, u32[]{:S(2)}) collective-permute-start(bf16[6,512]{1,0:T(8,128)(2,1)S(1)} %slice.38), channel_id=1, source_target_pairs={{0,1},{1,2},{2,3},{4,5},{5,6},{6,7},{8,9},{9,10},{10,11},{12,13},{... | collective-permute-start | bytes 18440
